TPU v7x, 512 devices: a whole 4x4x16 slice. The times are simulated.
512 devices in a mesh: fs: 64 (over z, y), tp: 8 (over x, core).
Axes of the slice: x: 4, y: 4, z: 16, core: 2. Of those that a mesh axis runs over, the one named last changes fastest.
Arguments:
- tokens: bfloat16 [16384, 2048], P('fs', 'tp'), may hold values from -16 to 16, as said below
- mix_gain: bfloat16 [2048], P('tp'), may hold values from 0.099609375 to 1.8984375
- query_weight: bfloat16 [2048, 512], P('fs', 'tp'), may hold values from -0.125 to 0.125
- key_weight: bfloat16 [2048, 512], P('fs', 'tp'), may hold values from -0.125 to 0.125
- value_weight: bfloat16 [2048, 1024], P('fs', 'tp'), may hold values from -0.125 to 0.125
- output_gate_weight: bfloat16 [2048, 1024], P('fs', 'tp'), may hold values from -0.125 to 0.125
- out_weight: bfloat16 [1024, 2048], P('tp', 'fs'), may hold values from -0.1875 to 0.1875
- head_rates: float32 [8], P('tp'), may hold values from 0 to 1, as said below
- block_scale: float32 [128], P('fs'), may hold values from 0.5 to 2
- ffn_gain: bfloat16 [2048], P('tp'), may hold values from 0.099609375 to 1.8984375
- ff_gate: bfloat16 [2048, 5632], P('fs', 'tp'), may hold values from -0.125 to 0.125
- ff_up: bfloat16 [2048, 5632], P('fs', 'tp'), may hold values from -0.125 to 0.125
- ff_down: bfloat16 [5632, 2048], P('tp', 'fs'), may hold values from -0.078125 to 0.078125
- final_gain: bfloat16 [2048], P('tp'), may hold values from 0.099609375 to 1.8984375
Outputs:
- layer_out: bfloat16 [16384, 2048], P('fs', 'tp')
Inputs may be any that keep to these rules, and one draw needn't show every extreme that they name: `tokens`: column blocks of the activations have different scales. `head_rates`: positive rates.
All inputs are finite; a program needn't handle non-finite values.
Results may differ from a plain program's by a relative error of at most 0.014.
Values may be sent and summed in bfloat16 or wider, within the bound.
A program may use at most 64 MiB of HBM per device.

v0:
```python
import jax
import jax.numpy as jnp
from jax import lax
from jax.sharding import Mesh
from jax.sharding import PartitionSpec as P

D = 2048
DK = 64
DV = 128
BLK = 128
SEQ_LEN = 256
FS = ("fs_0", "fs_1")
EPS = 1e-06
THETA = 10000.0


def gather_turned(arrays, axis, dims):
    turned = [jnp.moveaxis(a, dim, 0) for a, dim in zip(arrays, dims)]
    both = jnp.concatenate([t.reshape(len(t), -1) for t in turned], axis=1)
    filled, at, outs = (lax.all_gather(both, axis, axis=0, tiled=True), 0, [])
    for t, dim in zip(turned, dims):
        share = filled[:, at : at + t[0].size].reshape(-1, *t.shape[1:])
        outs.append(jnp.moveaxis(share, 0, dim))
        at += t[0].size
    return tuple(outs)


def sent_together(arrays, axis, dim, along):
    widths = [a.shape[along] for a in arrays]
    both = jnp.concatenate(arrays, axis=along)
    filled = lax.all_gather(both, axis, axis=dim, tiled=True)
    return tuple(jnp.split(filled, [sum(widths[:k]) for k in range(1, len(widths))], axis=along))


def laid_out(tiles, dim):
    lengths = list(tiles.shape[1:])
    lengths[dim] *= tiles.shape[0]
    return jnp.moveaxis(tiles, 0, dim).reshape(lengths)


def copy_for_each(shard, axis):
    size = lax.axis_size(axis)
    return lax.all_to_all(
        jnp.broadcast_to(shard[None], (size, *shard.shape)), axis, 0, 0, tiled=True
    )


def gather_directly(shard, axis, dim):
    return laid_out(copy_for_each(shard, axis), dim)


def gathered_by_axis(shard, axes, dim):
    filled = shard
    for number in range(len(axes) - 1, -1, -1):
        filled = lax.all_gather(filled, axes[number], axis=dim, tiled=True)
    return filled


def in_blocks(shard, dim, size):
    lengths = shard.shape
    tiles = shard.reshape(*lengths[:dim], size, lengths[dim] // size, *lengths[dim + 1 :])
    return jnp.moveaxis(tiles, dim, 0)


def sent_and_summed(shard, axis, dim):
    size = lax.axis_size(axis)
    tiles = lax.all_to_all(in_blocks(shard, dim, size), axis, 0, 0, tiled=True)
    return jnp.sum(tiles.astype(jnp.float32), axis=0)


def of_everyone(shard, axis):
    return copy_for_each(shard, axis).sum(axis=0)


def rms_norm(values, gain):
    scale = lax.rsqrt(jnp.mean(values * values, axis=-1, keepdims=True) + EPS)
    return values * scale * gain.astype(jnp.float32)


def rotate(values, positions):
    half = values.shape[-1] // 2
    inverse = THETA ** (-jnp.arange(half, dtype=jnp.float32) / half)
    angle = positions.astype(jnp.float32)[:, None] * inverse
    cosine = jnp.cos(angle)[:, None, :]
    sine = jnp.sin(angle)[:, None, :]
    first = values[..., :half]
    second = values[..., half:]
    return jnp.concatenate(
        [first * cosine - second * sine, second * cosine + first * sine], axis=-1
    )


def retain(query, key, value, rates, scales):
    rows, heads_here, width_k = query.shape
    width_v = value.shape[-1]
    nblk = rows // BLK
    hi = lax.Precision.HIGHEST
    qblk = query.astype(jnp.float32).reshape(nblk, BLK, heads_here, width_k)
    kblk = key.astype(jnp.float32).reshape(nblk, BLK, heads_here, width_k)
    vblk = value.astype(jnp.float32).reshape(nblk, BLK, heads_here, width_v)
    logdec = -rates[None, :] * scales[:, None]
    steps = jnp.arange(BLK, dtype=jnp.float32)
    offset = steps[:, None] - steps[None, :]
    causal = offset >= 0
    inside = jnp.where(
        causal[None, None],
        jnp.exp(logdec[:, :, None, None] * jnp.where(causal, offset, 0.0)[None, None]),
        0.0,
    )
    scores = jnp.einsum("nchd,nmhd->nhcm", qblk, kblk, precision=hi) * inside
    inner = jnp.einsum("nhcm,nmhe->nche", scores, vblk, precision=hi)
    zeta = jnp.exp(logdec[:, :, None] * (BLK - 1.0 - steps)[None, None, :])
    kv_block = jnp.einsum(
        "nchd,nche->nhde", kblk * jnp.transpose(zeta, (0, 2, 1))[..., None], vblk, precision=hi
    )
    hold = jnp.exp(logdec * BLK)
    per_seq = SEQ_LEN // BLK
    fresh = (jnp.arange(nblk, dtype=jnp.int32) % per_seq == 0).astype(jnp.float32)

    def advance(state, inputs):
        kv_now, hold_now, fresh_now = inputs
        before = state * (1.0 - fresh_now)
        return (before * hold_now[:, None, None] + kv_now, before)

    start = jnp.zeros((heads_here, width_k, width_v), jnp.float32)
    _, before = lax.scan(advance, start, (kv_block, hold, fresh))
    xi = jnp.exp(logdec[:, :, None] * (steps + 1.0)[None, None, :])
    cross = jnp.einsum(
        "nchd,nhde->nche", qblk * jnp.transpose(xi, (0, 2, 1))[..., None], before, precision=hi
    )
    total = inner + cross
    total = total * lax.rsqrt(jnp.mean(total * total, axis=-1, keepdims=True) + EPS)
    return total.reshape(rows, heads_here * width_v)


def body(
    tokens,
    mix_gain,
    query_weight,
    key_weight,
    value_weight,
    output_gate_weight,
    out_weight,
    head_rates,
    block_scale,
    ffn_gain,
    ff_gate,
    ff_up,
    ff_down,
    final_gain,
):
    rows = tokens.shape[0]
    heads_here = head_rates.shape[0]
    groups = lax.axis_size("tp")
    positions = jnp.arange(rows, dtype=jnp.int32) % SEQ_LEN
    whole, gain_whole = gather_turned((tokens, mix_gain), "tp", (1, 0))
    normed = rms_norm(whole.astype(jnp.float32), gain_whole).astype(jnp.bfloat16)
    collected = sent_together(
        (query_weight, key_weight, value_weight, output_gate_weight), FS, 0, 1
    )
    qproj, kproj, vproj, gproj = tuple(
        (jnp.dot(normed, weight, preferred_element_type=jnp.float32) for weight in collected)
    )
    query = rotate(qproj.reshape(rows, heads_here, DK), positions).astype(jnp.bfloat16)
    key = (rotate(kproj.reshape(rows, heads_here, DK), positions) * DK ** (-0.5)).astype(
        jnp.bfloat16
    )
    value = vproj.astype(jnp.bfloat16).reshape(rows, heads_here, DV)
    normret = retain(query, key, value, head_rates, block_scale)
    gated = (normret * jax.nn.silu(gproj)).astype(jnp.bfloat16)
    all_heads = gather_directly(gated, "tp", 1)
    head_rows = gathered_by_axis(out_weight, FS, 1)
    feature_block = lax.all_to_all(head_rows, "tp", split_axis=1, concat_axis=0, tiled=True)
    width = all_heads.shape[1] // groups
    left = all_heads.reshape(rows, groups, width)
    right = feature_block.reshape(groups, width, feature_block.shape[1])
    partial_sums = jnp.einsum(
        "rng,nge->nre", left, right, preferred_element_type=jnp.float32
    ).astype(jnp.bfloat16)
    mix = jnp.sum(partial_sums.astype(jnp.float32), axis=0)
    resid = (tokens.astype(jnp.float32) + mix).astype(jnp.bfloat16)
    whole2, gain2 = gather_turned((resid, ffn_gain), "tp", (1, 0))
    normed2 = rms_norm(whole2.astype(jnp.float32), gain2).astype(jnp.bfloat16)
    gate_rows, up_rows = sent_together((ff_gate, ff_up), FS, 0, 1)
    gate_part = jnp.dot(normed2, gate_rows, preferred_element_type=jnp.float32)
    up_part = jnp.dot(normed2, up_rows, preferred_element_type=jnp.float32)
    hidden = (jax.nn.silu(gate_part) * up_part).astype(jnp.bfloat16)
    down_terms = jnp.dot(
        hidden, gathered_by_axis(ff_down, FS, 1), preferred_element_type=jnp.float32
    )
    ffn = sent_and_summed(down_terms.astype(jnp.bfloat16), "tp", 1)
    total = resid.astype(jnp.float32) + ffn
    squares = of_everyone(jnp.sum(total * total, axis=-1, keepdims=True), "tp")
    scale = lax.rsqrt(squares / D + EPS)
    return (total * scale * final_gain.astype(jnp.float32)).astype(jnp.bfloat16)


def solution(mesh):
    finer = Mesh(mesh.devices.reshape(16, 4, mesh.shape["tp"]), ("fs_0", "fs_1", "tp"))
    return jax.shard_map(
        body,
        mesh=finer,
        in_specs=(
            P(FS, "tp"),
            P("tp"),
            P(FS, "tp"),
            P(FS, "tp"),
            P(FS, "tp"),
            P(FS, "tp"),
            P("tp", FS),
            P("tp"),
            P(FS),
            P("tp"),
            P(FS, "tp"),
            P(FS, "tp"),
            P("tp", FS),
            P("tp"),
        ),
        out_specs=P(FS, "tp"),
        check_vma=False,
    )
```

profile of v0, /device:TPU:1, one launch (start us, length us, event | category | flops | bytes accessed | tf_op | source)
XLA Modules:
  0.0 515.7 jit_solution(17452584656318330392)
XLA Ops:
  6.5 0.7 reshape.400
  7.2 1.6 pad_maximum_fusion
  8.9 1.4 pad_maximum_fusion.3
  10.3 10.6 %all_gather.26 = bf16[128,128]{0,1:T(8,128)(2,1)S(1)} all-gather(bf16[128,32]{0,1:T(8,128)(2,1)} %param.22), channel_id=1, replica_groups=mesh['fs_0'=16,'fs_1'=4,'tp'=8] {'fs_1'}, dimensions={1}, use_global_device_ids=true | all-gather | bytes 40960 | tf_op jit(solution)/shard_map/all_gather | solution.py:55
  20.9 31.9 %all_gather.27 = bf16[128,2048]{0,1:T(8,128)(2,1)S(1)} all-gather(bf16[128,128]{0,1:T(8,128)(2,1)S(1)} %all_gather.26), channel_id=1, replica_groups=mesh['fs_0'=16,'fs_1'=4,'tp'=8] {'fs_0'}, dimensions={1}, use_global_device_ids=true | all-gather | bytes 557056 | tf_op jit(solution)/shard_map/all_gather | solution.py:55
  52.8 1.0 copy.31
  53.8 14.1 %all-to-all-start.1 = ((bf16[128,8,256]{2,0,1:T(8,128)(2,1)}), bf16[128,8,256]{2,0,1:T(8,128)(2,1)S(1)}, u32[]{:S(2)}, u32[]{:S(2)}) async-start(bf16[128,8,256]{2,0,1:T(8,128)(2,1)} %copy.31), calls=%async_computation.1 | async-start | bytes 1048576 | tf_op jit(solution)/shard_map/all_to_all | solution.py:173
  68.9 1.6 fusion.4
  70.5 0.8 slice_convert_fusion.1
  71.2 109.0 %all-gather.8.cloned.1.call-done = bf16[2048,384]{1,0:T(8,128)(2,1)} async-done(((bf16[32,384]{1,0:T(8,128)(2,1)}), bf16[2048,384]{1,0:T(8,128)(2,1)}) %all-gather.8.cloned.1.call-update) | async-done | bytes 1572880 | tf_op jit(solution)/shard_map/all_gather | solution.py:31
  180.3 2.0 convolution_bitcast_fusion
  182.3 1.6 convolution_bitcast_fusion.1
  183.9 0.2 fusion.58
  184.2 1.5 convolution_convert_fusion.2
  185.8 0.2 convolution_bitcast_fusion.2
  185.9 5.0 while.13
  185.9 0.6 dynamic_slice.22
  187.2 0.6 constant_dynamic-slice_fusion.2
  187.8 0.7 bitcast_add_fusion.2
  188.5 0.6 dynamic_slice.22
  189.7 0.6 constant_dynamic-slice_fusion.2
  190.3 0.7 bitcast_add_fusion.2
  191.1 0.2 convolution_multiply_fusion
  191.3 0.2 fusion.74
  191.5 0.5 multiply_reduce_fusion.1
  192.0 0.1 broadcast_multiply_fusion
  192.1 1.6 fusion.35
  193.7 0.9 broadcast_in_dim.29
  194.6 15.1 %all-to-all-start = ((bf16[8,256,128]{2,1,0:T(8,128)(2,1)}), bf16[8,256,128]{2,1,0:T(8,128)(2,1)S(1)}, u32[]{:S(2)}, u32[]{:S(2)}) async-start(bf16[8,256,128]{2,1,0:T(8,128)(2,1)} %broadcast_in_dim.29), calls=%async_computation | async-start | bytes 1048576 | tf_op jit(solution)/shard_map/all_to_all | solution.py:43
  209.7 9.3 %all-to-all-done = bf16[8,256,128]{2,1,0:T(8,128)(2,1)S(1)} async-done(((bf16[8,256,128]{2,1,0:T(8,128)(2,1)}), bf16[8,256,128]{2,1,0:T(8,128)(2,1)S(1)}, u32[]{:S(2)}, u32[]{:S(2)}) %all-to-all-start) | async-done | bytes 524320 | tf_op jit(solution)/shard_map/all_to_all | solution.py:43
  219.0 0.4 convert_reduce_fusion.1
  219.5 0.7 pad_maximum_fusion.1
  220.3 0.7 pad_maximum_fusion.2
  221.1 10.0 %all_gather.30 = bf16[704,128]{0,1:T(8,128)(2,1)} all-gather(bf16[704,32]{0,1:T(8,128)(2,1)S(1)} %copy-done.5), channel_id=1, replica_groups=mesh['fs_0'=16,'fs_1'=4,'tp'=8] {'fs_1'}, dimensions={1}, use_global_device_ids=true | all-gather | bytes 225280 | tf_op jit(solution)/shard_map/all_gather | solution.py:55
  231.1 15.0 %all-gather.10.cloned.1.call-done = bf16[2048,257]{0,1:T(8,128)(2,1)} async-done(((bf16[256,257]{0,1:T(8,128)(2,1)}), bf16[2048,257]{0,1:T(8,128)(2,1)}) %all-gather.10.cloned.1.call-update) | async-done | bytes 1052688 | tf_op jit(solution)/shard_map/all_gather | solution.py:20
  246.0 1.5 fusion.7
  247.6 0.8 slice_convert_fusion
  248.3 142.7 %all-gather.12.cloned.1.call-done = bf16[2048,1408]{1,0:T(8,128)(2,1)} async-done(((bf16[32,1408]{1,0:T(8,128)(2,1)}), bf16[2048,1408]{1,0:T(8,128)(2,1)}) %all-gather.12.cloned.1.call-update) | async-done | bytes 5767184 | tf_op jit(solution)/shard_map/all_gather | solution.py:31
  391.0 3.7 fusion.2
  394.7 68.0 %all-gather.14.cloned.1.call-done = bf16[704,2048]{0,1:T(8,128)(2,1)} async-done(((bf16[704,128]{0,1:T(8,128)(2,1)}), bf16[704,2048]{0,1:T(8,128)(2,1)}) %all-gather.14.cloned.1.call-update) | async-done | bytes 2883600 | tf_op jit(solution)/shard_map/all_gather | solution.py:55
  462.7 7.2 %convolution_convert_fusion = bf16[256,2048]{1,0:T(8,128)(2,1)S(1)} fusion(bf16[704,2048]{0,1:T(8,128)(2,1)} %all-gather.14.cloned.1.call-done, bf16[2048,1408]{1,0:T(8,128)(2,1)} %all-gather.12.cloned.1.call-done, f32[256,704]{0,1:T(8,128)S(1)} %fusion.2, f32[2048]{0:T(1024)S(1)} %bitcast.82, f32[256]{0:T(256)S(1)} %add_rsqrt_fusion.1, ...), kind=kOutput, calls=%fused_computation.12 | convolution fusion | flops 1480097792 | bytes 9118720 | tf_op jit(solution)/shard_map/dot_general | solution.py:188
  470.1 28.6 %all_to_all.31 = bf16[8,256,256]{2,1,0:T(8,128)(2,1)S(1)} all-to-all(bf16[8,256,256]{2,1,0:T(8,128)(2,1)S(1)} %bitcast.70), channel_id=1, replica_groups=mesh['fs_0'=16,'fs_1'=4,'tp'=8] {'tp'}, dimensions={0} | all-to-all | bytes 2097152 | tf_op jit(solution)/shard_map/all_to_all | solution.py:67
  498.6 0.1 convert_reduce_fusion
  498.8 0.1 multiply_reduce_fusion
  498.9 0.6 broadcast_in_dim.30
  499.5 4.3 all-to-all-start.3
  503.8 4.6 all-to-all-done.3
  508.4 0.8 multiply_convert_fusion
  (59 shorter events, 0.7 us)
Async XLA Ops:
  6.5 62.2 %copy-start.6 = (f32[2]{0:T(128)S(1)}, f32[2]{0:T(128)}, u32[]{:S(2)}) copy-start(f32[2]{0:T(128)} %param.24) | copy-start | bytes 28
  6.5 62.3 %all-gather.6.cloned.1.call-start = ((), (), s32[]{:S(2)}) async-start(), calls=%async_computation.4 | async-start | bytes 1216512 | tf_op jit(solution)/shard_map/all_gather | solution.py:20
  8.8 171.5 %all-gather.8.cloned.1.call-start = ((), (), s32[]{:S(2)}) async-start(), calls=%async_computation.5 | async-start | bytes 1597440 | tf_op jit(solution)/shard_map/all_gather | solution.py:31
  53.8 139.9 %all-to-all-start.1 = ((bf16[128,8,256]{2,0,1:T(8,128)(2,1)}), bf16[128,8,256]{2,0,1:T(8,128)(2,1)S(1)}, u32[]{:S(2)}, u32[]{:S(2)}) async-start(bf16[128,8,256]{2,0,1:T(8,128)(2,1)} %copy.31), calls=%async_computation.1 | async-start | bytes 1048576 | tf_op jit(solution)/shard_map/all_to_all | solution.py:173
  68.9 113.5 %copy-start = (bf16[2048,257]{0,1:T(8,128)(2,1)S(1)}, bf16[2048,257]{0,1:T(8,128)(2,1)}, u32[]{:S(2)}) copy-start(bf16[2048,257]{0,1:T(8,128)(2,1)} %all-gather.6.cloned.1.call-done) | copy-start | bytes 3158020
  192.1 17.6 %copy-start.7 = (bf16[256]{0:T(256)(128)(2,1)S(1)}, bf16[256]{0:T(256)(128)(2,1)}, u32[]{:S(2)}) copy-start(bf16[256]{0:T(256)(128)(2,1)} %param.25) | copy-start | bytes 1540
  193.7 25.8 %copy-start.2 = (bf16[256,256]{1,0:T(8,128)(2,1)S(1)}, bf16[256,256]{1,0:T(8,128)(2,1)}, u32[]{:S(2)}) copy-start(bf16[256,256]{1,0:T(8,128)(2,1)} %param.16) | copy-start | bytes 393220
  193.7 26.6 %copy-start.3 = (bf16[32,704]{1,0:T(8,128)(2,1)S(1)}, bf16[32,704]{1,0:T(8,128)(2,1)}, u32[]{:S(2)}) copy-start(bf16[32,704]{1,0:T(8,128)(2,1)} %param.27) | copy-start | bytes 135172
  193.7 26.6 %copy-start.4 = (bf16[32,704]{1,0:T(8,128)(2,1)S(1)}, bf16[32,704]{1,0:T(8,128)(2,1)}, u32[]{:S(2)}) copy-start(bf16[32,704]{1,0:T(8,128)(2,1)} %param.26) | copy-start | bytes 135172
  193.7 27.3 %copy-start.5 = (bf16[704,32]{0,1:T(8,128)(2,1)S(1)}, bf16[704,32]{0,1:T(8,128)(2,1)}, u32[]{:S(2)}) copy-start(bf16[704,32]{0,1:T(8,128)(2,1)} %param.28) | copy-start | bytes 135172
  194.6 24.4 %all-to-all-start = ((bf16[8,256,128]{2,1,0:T(8,128)(2,1)}), bf16[8,256,128]{2,1,0:T(8,128)(2,1)S(1)}, u32[]{:S(2)}, u32[]{:S(2)}) async-start(bf16[8,256,128]{2,1,0:T(8,128)(2,1)} %broadcast_in_dim.29), calls=%async_computation | async-start | bytes 1048576 | tf_op jit(solution)/shard_map/all_to_all | solution.py:43
  209.7 36.4 %all-gather.10.cloned.1.call-start = ((), (), s32[]{:S(2)}) async-start(), calls=%async_computation.6 | async-start | bytes 1216512 | tf_op jit(solution)/shard_map/all_gather | solution.py:20
  220.2 170.8 %all-gather.12.cloned.1.call-start = ((), (), s32[]{:S(2)}) async-start(), calls=%async_computation.7 | async-start | bytes 5857280 | tf_op jit(solution)/shard_map/all_gather | solution.py:31
  221.0 241.7 %all-gather.14.cloned.1.call-start = ((), (), s32[]{:S(2)}) async-start(), calls=%async_computation.8 | async-start | bytes 3342336 | tf_op jit(solution)/shard_map/all_gather | solution.py:55
  391.0 71.7 %copy-start.1 = (bf16[2048,257]{0,1:T(8,128)(2,1)S(1)}, bf16[2048,257]{0,1:T(8,128)(2,1)}, u32[]{:S(2)}) copy-start(bf16[2048,257]{0,1:T(8,128)(2,1)} %all-gather.10.cloned.1.call-done) | copy-start | bytes 3158020
  470.0 33.7 %copy-start.8 = (bf16[256]{0:T(256)(128)(2,1)S(1)}, bf16[256]{0:T(256)(128)(2,1)}, u32[]{:S(2)}) copy-start(bf16[256]{0:T(256)(128)(2,1)} %param.29) | copy-start | bytes 1540
  499.5 8.9 %all-to-all-start.3 = ((f32[8,256,1]{1,2,0:T(1,128)}), f32[8,256,1]{1,2,0:T(1,128)S(1)}, u32[]{:S(2)}, u32[]{:S(2)}) async-start(f32[8,256,1]{1,2,0:T(1,128)} %broadcast_in_dim.30), calls=%async_computation.3 | async-start | bytes 16384 | tf_op jit(solution)/shard_map/all_to_all | solution.py:43
Sparse Core Ops, SparseCore 0:
  9.4 36.6 all-gather.5
  49.1 131.1 all-gather.7
  220.3 25.6 all-gather.9
  248.8 142.1 all-gather.11
  392.9 69.7 all-gather.13
where the time goes:
time: 517 us; the launch traced here: 516 us
  waiting for transfers between devices  349 us (68%)
  blocking collectives  81 us (16%)
  starting transfers between devices  33.6 us (6%)
  matrix products  19.1 us (4%)
  between operations  14.1 us (3%)
  other arithmetic  12 us (2%)
  local copies, waits for them, and re-layouts  5.72 us (1%)
    all_gather x2, waiting for transfers between devices, sent_together(): filled = lax.all_gather(both, axis, axis=dim, tiled=True)  252 us
    all_gather x1, waiting for transfers between devices, gathered_by_axis(): filled = lax.all_gather(filled, axes[number], axis=dim, tiled=True)  68 us
    all_gather x3, blocking collectives, gathered_by_axis(): filled = lax.all_gather(filled, axes[number], axis=dim, tiled=True)  52.5 us
    all_to_all x1, blocking collectives, sent_and_summed(): tiles = lax.all_to_all(in_blocks(shard, dim, size), axis, 0, 0, tiled=True)  28.6 us
    all_to_all x2, starting transfers between devices, copy_for_each(): lax.all_to_all(jnp.broadcast_to(shard[None], (size, *shard.shape)), axis,...  19.4 us
    all_gather x2, waiting for transfers between devices, gather_turned(): filled, at, outs = (lax.all_gather(both, axis, axis=0, tiled=True), 0, [])  15 us
    all_to_all x1, starting transfers between devices, body(): lax.all_to_all(head_rows, 'tp', split_axis=1, concat_axis=0, tiled=True)  14.1 us
    all_to_all x2, waiting for transfers between devices, copy_for_each(): lax.all_to_all(jnp.broadcast_to(shard[None], (size, *shard.shape)), axis,...  14 us
  transfers between devices with their start and end apart: 8, of which 6 were waited for; matrix products, arithmetic and copies ran while one was open for 5% of the time, Pallas kernels for 0%

commit v1 on v0

--- a/solution.py
+++ b/solution.py
@@ -170,7 +170,10 @@
     gated = (normret * jax.nn.silu(gproj)).astype(jnp.bfloat16)
     all_heads = gather_directly(gated, "tp", 1)
     head_rows = gathered_by_axis(out_weight, FS, 1)
-    feature_block = lax.all_to_all(head_rows, "tp", split_axis=1, concat_axis=0, tiled=True)
+    feature_block = jnp.concatenate(
+        lax.all_to_all(jnp.stack(jnp.split(head_rows, lax.axis_size("tp"), axis=1)), "tp", 0, 0),
+        axis=0,
+    )
     width = all_heads.shape[1] // groups
     left = all_heads.reshape(rows, groups, width)
     right = feature_block.reshape(groups, width, feature_block.shape[1])

time: 517 us -> 517 us (level)
  no operation moved by 1% of the time
where the time goes in v1:
time: 517 us; the launch traced here: 516 us
  waiting for transfers between devices  345 us (67%)
  blocking collectives  81 us (16%)
  starting transfers between devices  33.6 us (6%)
  matrix products  19.1 us (4%)
  between operations  14.1 us (3%)
  other arithmetic  12 us (2%)
  local copies, waits for them, and re-layouts  9.81 us (2%)
    all_gather x2, waiting for transfers between devices, sent_together(): filled = lax.all_gather(both, axis, axis=dim, tiled=True)  248 us
    all_gather x1, waiting for transfers between devices, gathered_by_axis(): filled = lax.all_gather(filled, axes[number], axis=dim, tiled=True)  68 us
    all_gather x3, blocking collectives, gathered_by_axis(): filled = lax.all_gather(filled, axes[number], axis=dim, tiled=True)  52.5 us
    all_to_all x1, blocking collectives, sent_and_summed(): tiles = lax.all_to_all(in_blocks(shard, dim, size), axis, 0, 0, tiled=True)  28.6 us
    all_to_all x2, starting transfers between devices, copy_for_each(): lax.all_to_all(jnp.broadcast_to(shard[None], (size, *shard.shape)), axis,...  19.4 us
    all_gather x2, waiting for transfers between devices, gather_turned(): filled, at, outs = (lax.all_gather(both, axis, axis=0, tiled=True), 0, [])  15 us
    all_to_all x1, starting transfers between devices, body(): lax.all_to_all(jnp.stack(jnp.split(head_rows, lax.axis_size('tp'), axis=1...  14.1 us
    all_to_all x2, waiting for transfers between devices, copy_for_each(): lax.all_to_all(jnp.broadcast_to(shard[None], (size, *shard.shape)), axis,...  14 us
  transfers between devices with their start and end apart: 8, of which 6 were waited for; matrix products, arithmetic and copies ran while one was open for 5% of the time, Pallas kernels for 0%

profile of v1, /device:TPU:1, one launch (start us, length us, event | category | flops | bytes accessed | tf_op | source)
XLA Modules:
  0.0 515.8 jit_solution(14410864325760942766)
XLA Ops:
  6.5 0.7 reshape.395
  7.2 1.6 pad_maximum_fusion
  8.9 1.4 pad_maximum_fusion.3
  10.3 10.6 %all_gather.26 = bf16[128,128]{0,1:T(8,128)(2,1)S(1)} all-gather(bf16[128,32]{0,1:T(8,128)(2,1)} %param.22), channel_id=1, replica_groups=mesh['fs_0'=16,'fs_1'=4,'tp'=8] {'fs_1'}, dimensions={1}, use_global_device_ids=true | all-gather | bytes 40960 | tf_op jit(solution)/shard_map/all_gather | solution.py:55
  21.0 31.9 %all_gather.27 = bf16[128,2048]{1,0:T(8,128)(2,1)S(1)} all-gather(bf16[128,128]{1,0:T(8,128)(2,1)S(1)} %copy.26), channel_id=1, replica_groups=mesh['fs_0'=16,'fs_1'=4,'tp'=8] {'fs_0'}, dimensions={1}, use_global_device_ids=true | all-gather | bytes 557056 | tf_op jit(solution)/shard_map/all_gather | solution.py:55
  52.9 0.6 fusion.44
  53.6 0.6 fusion.43
  54.2 0.6 fusion.42
  54.8 0.6 fusion.41
  55.4 0.6 fusion.40
  56.1 0.6 fusion.39
  56.7 0.6 fusion.38
  57.3 0.6 fusion.37
  58.0 14.1 %all-to-all-start.1 = ((bf16[8,128,256]{2,1,0:T(8,128)(2,1)}), bf16[8,128,256]{2,1,0:T(8,128)(2,1)S(1)}, u32[]{:S(2)}, u32[]{:S(2)}) async-start(bf16[8,128,256]{2,1,0:T(8,128)(2,1)} %fusion.37), calls=%async_computation.1 | async-start | bytes 1048576 | tf_op jit(solution)/shard_map/all_to_all | solution.py:174
  73.0 1.6 fusion.4
  74.6 0.8 slice_convert_fusion.1
  75.4 105.0 %all-gather.8.cloned.1.call-done = bf16[2048,384]{1,0:T(8,128)(2,1)} async-done(((bf16[32,384]{1,0:T(8,128)(2,1)}), bf16[2048,384]{1,0:T(8,128)(2,1)}) %all-gather.8.cloned.1.call-update) | async-done | bytes 1572880 | tf_op jit(solution)/shard_map/all_gather | solution.py:31
  180.3 2.0 convolution_bitcast_fusion
  182.4 1.6 convolution_bitcast_fusion.1
  184.6 1.5 convolution_convert_fusion.2
  186.5 5.0 while.13
  186.5 0.6 dynamic_slice.22
  187.8 0.6 constant_dynamic-slice_fusion.2
  188.4 0.7 bitcast_add_fusion.2
  189.0 0.6 dynamic_slice.22
  190.3 0.6 constant_dynamic-slice_fusion.2
  190.9 0.7 bitcast_add_fusion.2
  191.6 0.5 multiply_reduce_fusion.1
  192.2 1.6 fusion.34
  193.8 0.9 broadcast_in_dim.29
  194.6 15.1 %all-to-all-start = ((bf16[8,256,128]{2,1,0:T(8,128)(2,1)}), bf16[8,256,128]{2,1,0:T(8,128)(2,1)S(1)}, u32[]{:S(2)}, u32[]{:S(2)}) async-start(bf16[8,256,128]{2,1,0:T(8,128)(2,1)} %broadcast_in_dim.29), calls=%async_computation | async-start | bytes 1048576 | tf_op jit(solution)/shard_map/all_to_all | solution.py:43
  209.7 9.3 %all-to-all-done = bf16[8,256,128]{2,1,0:T(8,128)(2,1)S(1)} async-done(((bf16[8,256,128]{2,1,0:T(8,128)(2,1)}), bf16[8,256,128]{2,1,0:T(8,128)(2,1)S(1)}, u32[]{:S(2)}, u32[]{:S(2)}) %all-to-all-start) | async-done | bytes 524320 | tf_op jit(solution)/shard_map/all_to_all | solution.py:43
  219.1 0.4 convert_reduce_fusion.1
  219.6 0.7 pad_maximum_fusion.1
  220.3 0.7 pad_maximum_fusion.2
  221.1 10.0 %all_gather.30 = bf16[704,128]{0,1:T(8,128)(2,1)} all-gather(bf16[704,32]{0,1:T(8,128)(2,1)S(1)} %copy-done.5), channel_id=1, replica_groups=mesh['fs_0'=16,'fs_1'=4,'tp'=8] {'fs_1'}, dimensions={1}, use_global_device_ids=true | all-gather | bytes 225280 | tf_op jit(solution)/shard_map/all_gather | solution.py:55
  231.1 15.0 %all-gather.10.cloned.1.call-done = bf16[2048,257]{0,1:T(8,128)(2,1)} async-done(((bf16[256,257]{0,1:T(8,128)(2,1)}), bf16[2048,257]{0,1:T(8,128)(2,1)}) %all-gather.10.cloned.1.call-update) | async-done | bytes 1052688 | tf_op jit(solution)/shard_map/all_gather | solution.py:20
  246.1 1.5 fusion.7
  247.6 0.8 slice_convert_fusion
  248.4 142.7 %all-gather.12.cloned.1.call-done = bf16[2048,1408]{1,0:T(8,128)(2,1)} async-done(((bf16[32,1408]{1,0:T(8,128)(2,1)}), bf16[2048,1408]{1,0:T(8,128)(2,1)}) %all-gather.12.cloned.1.call-update) | async-done | bytes 5767184 | tf_op jit(solution)/shard_map/all_gather | solution.py:31
  391.1 3.7 fusion.2
  394.7 68.0 %all-gather.14.cloned.1.call-done = bf16[704,2048]{0,1:T(8,128)(2,1)} async-done(((bf16[704,128]{0,1:T(8,128)(2,1)}), bf16[704,2048]{0,1:T(8,128)(2,1)}) %all-gather.14.cloned.1.call-update) | async-done | bytes 2883600 | tf_op jit(solution)/shard_map/all_gather | solution.py:55
  462.8 7.2 %convolution_convert_fusion = bf16[256,2048]{1,0:T(8,128)(2,1)S(1)} fusion(bf16[704,2048]{0,1:T(8,128)(2,1)} %all-gather.14.cloned.1.call-done, bf16[2048,1408]{1,0:T(8,128)(2,1)} %all-gather.12.cloned.1.call-done, f32[256,704]{0,1:T(8,128)S(1)} %fusion.2, f32[2048]{0:T(1024)S(1)} %bitcast.110, f32[256]{0:T(256)S(1)} %add_rsqrt_fusion.1, ...), kind=kOutput, calls=%fused_computation.12 | convolution fusion | flops 1480097792 | bytes 9118720 | tf_op jit(solution)/shard_map/dot_general | solution.py:191
  470.1 28.6 %all_to_all.20 = bf16[8,256,256]{2,1,0:T(8,128)(2,1)S(1)} all-to-all(bf16[8,256,256]{2,1,0:T(8,128)(2,1)S(1)} %bitcast.99), channel_id=1, replica_groups=mesh['fs_0'=16,'fs_1'=4,'tp'=8] {'tp'}, dimensions={0} | all-to-all | bytes 2097152 | tf_op jit(solution)/shard_map/all_to_all | solution.py:67
  498.9 0.6 broadcast_in_dim.30
  499.5 4.3 all-to-all-start.3
  503.8 4.6 all-to-all-done.3
  508.5 0.8 multiply_convert_fusion
  (67 shorter events, 2.0 us)
Async XLA Ops:
  6.5 66.3 %copy-start.6 = (f32[2]{0:T(128)S(1)}, f32[2]{0:T(128)}, u32[]{:S(2)}) copy-start(f32[2]{0:T(128)} %param.24) | copy-start | bytes 28
  6.5 66.4 %all-gather.6.cloned.1.call-start = ((), (), s32[]{:S(2)}) async-start(), calls=%async_computation.4 | async-start | bytes 1216512 | tf_op jit(solution)/shard_map/all_gather | solution.py:20
  8.8 171.5 %all-gather.8.cloned.1.call-start = ((), (), s32[]{:S(2)}) async-start(), calls=%async_computation.5 | async-start | bytes 1597440 | tf_op jit(solution)/shard_map/all_gather | solution.py:31
  58.0 135.8 %all-to-all-start.1 = ((bf16[8,128,256]{2,1,0:T(8,128)(2,1)}), bf16[8,128,256]{2,1,0:T(8,128)(2,1)S(1)}, u32[]{:S(2)}, u32[]{:S(2)}) async-start(bf16[8,128,256]{2,1,0:T(8,128)(2,1)} %fusion.37), calls=%async_computation.1 | async-start | bytes 1048576 | tf_op jit(solution)/shard_map/all_to_all | solution.py:174
  73.0 109.4 %copy-start = (bf16[2048,257]{0,1:T(8,128)(2,1)S(1)}, bf16[2048,257]{0,1:T(8,128)(2,1)}, u32[]{:S(2)}) copy-start(bf16[2048,257]{0,1:T(8,128)(2,1)} %all-gather.6.cloned.1.call-done) | copy-start | bytes 3158020
  192.2 17.6 %copy-start.7 = (bf16[256]{0:T(256)(128)(2,1)S(1)}, bf16[256]{0:T(256)(128)(2,1)}, u32[]{:S(2)}) copy-start(bf16[256]{0:T(256)(128)(2,1)} %param.25) | copy-start | bytes 1540
  193.7 25.8 %copy-start.2 = (bf16[256,256]{1,0:T(8,128)(2,1)S(1)}, bf16[256,256]{1,0:T(8,128)(2,1)}, u32[]{:S(2)}) copy-start(bf16[256,256]{1,0:T(8,128)(2,1)} %param.16) | copy-start | bytes 393220
  193.7 26.6 %copy-start.3 = (bf16[32,704]{1,0:T(8,128)(2,1)S(1)}, bf16[32,704]{1,0:T(8,128)(2,1)}, u32[]{:S(2)}) copy-start(bf16[32,704]{1,0:T(8,128)(2,1)} %param.27) | copy-start | bytes 135172
  193.8 26.6 %copy-start.4 = (bf16[32,704]{1,0:T(8,128)(2,1)S(1)}, bf16[32,704]{1,0:T(8,128)(2,1)}, u32[]{:S(2)}) copy-start(bf16[32,704]{1,0:T(8,128)(2,1)} %param.26) | copy-start | bytes 135172
  193.8 27.3 %copy-start.5 = (bf16[704,32]{0,1:T(8,128)(2,1)S(1)}, bf16[704,32]{0,1:T(8,128)(2,1)}, u32[]{:S(2)}) copy-start(bf16[704,32]{0,1:T(8,128)(2,1)} %param.28) | copy-start | bytes 135172
  194.6 24.4 %all-to-all-start = ((bf16[8,256,128]{2,1,0:T(8,128)(2,1)}), bf16[8,256,128]{2,1,0:T(8,128)(2,1)S(1)}, u32[]{:S(2)}, u32[]{:S(2)}) async-start(bf16[8,256,128]{2,1,0:T(8,128)(2,1)} %broadcast_in_dim.29), calls=%async_computation | async-start | bytes 1048576 | tf_op jit(solution)/shard_map/all_to_all | solution.py:43
  209.7 36.4 %all-gather.10.cloned.1.call-start = ((), (), s32[]{:S(2)}) async-start(), calls=%async_computation.6 | async-start | bytes 1216512 | tf_op jit(solution)/shard_map/all_gather | solution.py:20
  220.2 170.8 %all-gather.12.cloned.1.call-start = ((), (), s32[]{:S(2)}) async-start(), calls=%async_computation.7 | async-start | bytes 5857280 | tf_op jit(solution)/shard_map/all_gather | solution.py:31
  221.1 241.7 %all-gather.14.cloned.1.call-start = ((), (), s32[]{:S(2)}) async-start(), calls=%async_computation.8 | async-start | bytes 3342336 | tf_op jit(solution)/shard_map/all_gather | solution.py:55
  391.1 71.7 %copy-start.1 = (bf16[2048,257]{0,1:T(8,128)(2,1)S(1)}, bf16[2048,257]{0,1:T(8,128)(2,1)}, u32[]{:S(2)}) copy-start(bf16[2048,257]{0,1:T(8,128)(2,1)} %all-gather.10.cloned.1.call-done) | copy-start | bytes 3158020
  470.1 33.7 %copy-start.8 = (bf16[256]{0:T(256)(128)(2,1)S(1)}, bf16[256]{0:T(256)(128)(2,1)}, u32[]{:S(2)}) copy-start(bf16[256]{0:T(256)(128)(2,1)} %param.29) | copy-start | bytes 1540
  499.5 8.9 %all-to-all-start.3 = ((f32[8,256,1]{1,2,0:T(1,128)}), f32[8,256,1]{1,2,0:T(1,128)S(1)}, u32[]{:S(2)}, u32[]{:S(2)}) async-start(f32[8,256,1]{1,2,0:T(1,128)} %broadcast_in_dim.30), calls=%async_computation.3 | async-start | bytes 16384 | tf_op jit(solution)/shard_map/all_to_all | solution.py:43
Sparse Core Ops, SparseCore 0:
  9.4 36.6 all-gather.5
  49.1 131.1 all-gather.7
  220.4 25.6 all-gather.9
  248.9 142.1 all-gather.11
  393.0 69.7 all-gather.13
